TPU v7x, 32 devices: a whole 2x2x4 slice. The times are simulated.
32 devices in a mesh: sp: 4 (over y, x), tp: 8 (over z, core).
Axes of the slice: x: 2, y: 2, z: 4, core: 2. Of those that a mesh axis runs over, the one named last changes fastest.
Arguments:
- tokens: bfloat16 [2048, 2048], P(('sp', 'tp')), may hold values from -6 to 6
- query_vectors: bfloat16 [2048, 2048], P('sp', 'tp'), may hold values from -8 to 8
- key_vectors: bfloat16 [2048, 2048], P('sp', 'tp'), may hold values from -8 to 8
- value_vectors: bfloat16 [2048, 2048], P('sp', 'tp'), may hold values from -24 to 24
- cum_gate: float32 [2048, 32], P('sp', 'tp'), may hold values from -260 to 0, as said below
- out_weight: bfloat16 [2048, 2048], P('tp'), may hold values from -0.125 to 0.125
- norm_gain: float32 [2048], replicated, may hold values from 0.1 to 1.9
- gate_weight: bfloat16 [4, 2048, 7168], P('sp', None, 'tp'), may hold values from -0.125 to 0.125
- up_weight: bfloat16 [4, 2048, 7168], P('sp', None, 'tp'), may hold values from -0.125 to 0.125
- down_weight: bfloat16 [4, 7168, 2048], P('sp', 'tp'), may hold values from -0.0625 to 0.0625
- expert_ids: int32 [2048, 2], P(('sp', 'tp')), may hold values from 0 to 3, all different within a row; in each aligned block of 64 rows (0 to 63, 64 to 127, ...) at most 48 rows name the same one
- route_weights: float32 [2048, 2], P(('sp', 'tp')), may hold values from 0.2 to 1
Outputs:
- layer_output: bfloat16 [2048, 2048], P(('sp', 'tp'))
Inputs may be any that keep to these rules, and one draw needn't show every extreme that they name: `cum_gate`: along the positions each head's values never rise. `expert_ids`: within the rows of one device no expert is named by more than 48 rows, and in some devices' rows one expert is named by exactly 48; a row names 2 different experts.
All inputs are finite; a program needn't handle non-finite values.
Results may differ from a plain program's by a relative error of at most 0.014.
Values may be sent and summed in bfloat16 or wider, within the bound.
A program may use at most 128 MiB of HBM per device.

v0:
```python
import math
import jax
import jax.numpy as jnp
from jax import lax
from jax.sharding import PartitionSpec as P

NEG_LARGE = -1e30


def shards(
    tokens,
    query_vectors,
    key_vectors,
    value_vectors,
    cum_gate,
    out_weight,
    norm_gain,
    gate_weight,
    up_weight,
    down_weight,
    expert_ids,
    route_weights,
):
    sp_count = lax.axis_size("sp")
    seg_rows = query_vectors.shape[0]
    heads_here = cum_gate.shape[1]
    head_width = query_vectors.shape[1] // heads_here
    score_scale = head_width ** (-0.5)
    offset = lax.axis_index("sp") * seg_rows
    last_query = offset + seg_rows - 1
    query_pos = offset + jnp.arange(seg_rows, dtype=jnp.int32)
    query_heads = query_vectors.reshape(seg_rows, heads_here, head_width)
    query_gate = cum_gate.T
    gate_rows = lax.all_gather(cum_gate, "sp", axis=0, tiled=True)

    def attend_block(carried, key_block, value_block, block_start):
        running_peak, running_total, accumulated = carried
        row_count = key_block.shape[0]
        key_heads = key_block.reshape(row_count, heads_here, head_width)
        value_heads = value_block.reshape(row_count, heads_here, head_width)
        key_gate = lax.dynamic_slice_in_dim(gate_rows, block_start, row_count, 0).T
        scores = (
            jnp.einsum("qhd,khd->hqk", query_heads, key_heads, preferred_element_type=jnp.float32)
            * score_scale
        )
        scores = scores + query_gate[:, :, None] - key_gate[:, None, :]
        key_pos = block_start + jnp.arange(row_count, dtype=jnp.int32)
        visible = (key_pos[None, :] <= query_pos[:, None])[None]
        scores = jnp.where(visible, scores, NEG_LARGE)
        new_peak = jnp.maximum(running_peak, jnp.max(scores, axis=2))
        exponent = jnp.where(visible, jnp.exp(scores - new_peak[:, :, None]), 0.0)
        rescale = jnp.exp(running_peak - new_peak)
        running_total = running_total * rescale + jnp.sum(exponent, axis=2)
        weighted = jnp.einsum(
            "hqk,khd->hqd",
            exponent.astype(jnp.bfloat16),
            value_heads,
            preferred_element_type=jnp.float32,
        )
        accumulated = accumulated * rescale[:, :, None] + weighted
        return (new_peak, running_total, accumulated)

    start_state = (
        jnp.full((heads_here, seg_rows), NEG_LARGE, jnp.float32),
        jnp.zeros((heads_here, seg_rows), jnp.float32),
        jnp.zeros((heads_here, seg_rows, head_width), jnp.float32),
    )
    carried = start_state
    key_piece = lax.all_gather(key_vectors, "sp", axis=0, tiled=True)
    value_piece = lax.all_gather(value_vectors, "sp", axis=0, tiled=True)
    row_count = key_piece.shape[0]
    block_rows = math.gcd(row_count, 1024)
    block_count = row_count // block_rows
    key_stack = key_piece.reshape(block_count, block_rows, key_piece.shape[1])
    value_stack = value_piece.reshape(block_count, block_rows, value_piece.shape[1])

    def step_block(state, inputs):
        key_block, value_block, block_index = inputs
        block_start = block_index * block_rows

        def take_block(inner):
            return attend_block(inner, key_block, value_block, block_start)

        def skip_block(inner):
            return inner

        return (lax.cond(block_start <= last_query, take_block, skip_block, state), None)

    carried, _ = lax.scan(
        step_block, carried, (key_stack, value_stack, jnp.arange(block_count, dtype=jnp.int32))
    )
    final_peak, final_total, accumulated = carried
    attended = (accumulated / final_total[:, :, None]).astype(jnp.bfloat16)
    attended = attended.transpose(1, 0, 2).reshape(seg_rows, heads_here * head_width)
    tok_dev = tokens.shape[0]
    model_width = tokens.shape[1]
    token_rows = lax.all_to_all(attended, "tp", split_axis=0, concat_axis=1, tiled=True)
    projected = jnp.dot(
        token_rows,
        lax.all_gather(out_weight, "tp", axis=0, tiled=True),
        preferred_element_type=jnp.float32,
    )
    stream_wide = (tokens.astype(jnp.float32) + projected).astype(jnp.bfloat16).astype(jnp.float32)
    inverse = lax.rsqrt(jnp.mean(stream_wide * stream_wide, axis=1, keepdims=True) + 1e-05)
    normed = (stream_wide * inverse * norm_gain[None, :]).astype(jnp.bfloat16)
    n_experts = gate_weight.shape[0] * sp_count
    top_count = expert_ids.shape[1]
    capacity = max(2, 3 * tok_dev * top_count // (2 * n_experts))
    flat_ids = expert_ids.reshape(-1)
    hits = (flat_ids[:, None] == jnp.arange(n_experts, dtype=jnp.int32)[None, :]).astype(jnp.int32)
    earlier = jnp.cumsum(hits, axis=0) - hits
    slot_index = flat_ids * capacity + jnp.sum(earlier * hits, axis=1)
    placement_map = (
        jnp.arange(n_experts * capacity, dtype=jnp.int32)[:, None] == slot_index[None, :]
    ).astype(jnp.bfloat16)
    repeated = jnp.repeat(normed, top_count, axis=0)
    dispatch = jnp.dot(placement_map, repeated, preferred_element_type=jnp.float32).astype(
        jnp.bfloat16
    )
    dispatch = dispatch.reshape(n_experts, capacity, model_width)
    arrived = lax.all_to_all(dispatch, "sp", split_axis=0, concat_axis=0, tiled=True)
    row_block = arrived.reshape(-1, model_width)
    rows_in = lax.all_gather(row_block, "tp", axis=0, tiled=True)
    gate_value = jnp.dot(rows_in, gate_weight[0], preferred_element_type=jnp.float32)
    up_value = jnp.dot(rows_in, up_weight[0], preferred_element_type=jnp.float32)
    hidden = (jax.nn.silu(gate_value) * up_value).astype(jnp.bfloat16)
    summed = lax.psum_scatter(
        jnp.dot(hidden, down_weight[0], preferred_element_type=jnp.float32).astype(jnp.bfloat16),
        "tp",
        scatter_dimension=0,
        tiled=True,
    )
    returned = summed.reshape(arrived.shape)
    back = lax.all_to_all(returned, "sp", split_axis=0, concat_axis=0, tiled=True)
    flat_back = back.reshape(n_experts * capacity, model_width)
    picked = flat_back[slot_index].astype(jnp.float32).reshape(tok_dev, top_count, model_width)
    mixture = jnp.sum(picked * route_weights[:, :, None], axis=1)
    return (stream_wide + mixture).astype(jnp.bfloat16)


def solution(mesh):
    in_specs = (
        P(("sp", "tp"), None),
        P("sp", "tp"),
        P("sp", "tp"),
        P("sp", "tp"),
        P("sp", "tp"),
        P("tp", None),
        P(),
        P("sp", None, "tp"),
        P("sp", None, "tp"),
        P("sp", "tp", None),
        P(("sp", "tp"), None),
        P(("sp", "tp"), None),
    )
    out_specs = P(("sp", "tp"), None)
    return jax.shard_map(shards, mesh=mesh, in_specs=in_specs, out_specs=out_specs, check_vma=False)
```

profile of v0, /device:TPU:0, one launch (start us, length us, event | category | flops | bytes accessed | tf_op | source)
XLA Modules:
  0.0 362.4 jit_solution(4247297287543457111)
XLA Ops:
  6.5 0.7 all-gather.5.cloned.1.call-update
  7.3 0.7 all-gather.7.cloned.1.call-update
  8.1 0.7 all-gather.9.cloned.1.call-update
  8.7 1.1 copy.27
  9.8 0.8 copy.32
  10.8 9.8 %all_gather.16 = f32[2048,4]{0,1:T(4,128)S(1)} all-gather(f32[512,4]{0,1:T(4,128)} %param.20), channel_id=1, replica_groups=mesh['sp'=4,'tp'=8] {'sp'}, dimensions={0}, use_global_device_ids=true | all-gather | bytes 40960 | tf_op jit(solution)/shard_map/all_gather | solution.py:34
  20.6 17.9 %all-gather.5.cloned.1.call-done = bf16[2048,256]{1,0:T(8,128)(2,1)} async-done(((bf16[512,256]{1,0:T(8,128)(2,1)}), bf16[2048,256]{1,0:T(8,128)(2,1)}) %all-gather.5.cloned.1.call-update) | async-done | bytes 1048592 | tf_op jit(solution)/shard_map/all_gather | solution.py:69
  38.4 1.5 copy.28
  39.9 26.9 %all-gather.7.cloned.1.call-done = bf16[2048,256]{1,0:T(8,128)(2,1)} async-done(((bf16[512,256]{1,0:T(8,128)(2,1)}), bf16[2048,256]{1,0:T(8,128)(2,1)}) %all-gather.7.cloned.1.call-update) | async-done | bytes 1048592 | tf_op jit(solution)/shard_map/all_gather | solution.py:70
  66.8 1.5 copy.29
  68.4 12.0 %while.15 = (s32[]{:T(128)}, f32[4,512]{1,0:T(4,128)S(1)}, f32[4,512]{1,0:T(4,128)S(1)}, f32[4,512,64]{1,2,0:T(8,128)S(1)}, s32[2]{0:T(128)S(1)}, /*index=5*/s32...) while((s32[]{:T(128)}, f32[4,512]{1,0:T(4,128)S(1)}, ...), condition=%wide.region_5.6_spmd.clone, body=%wide.region_0.5_spmd.clone.sunk | while | flops 577508864 | bytes 31973748 | solution.py:89
  68.4 0.7 dynamic_slice.31
  69.8 9.2 %conditional.3 = ((f32[4,512]{1,0:T(4,128)S(1)}, f32[4,512]{1,0:T(4,128)S(1)}, f32[4,512,64]{1,2,0:T(8,128)S(1)})) conditional(s32[]{:T(128)} %convert_element_type.83, (f32[4,512]{1,0:T(4,128)S(1)}, f32[4,512]{1,0:T(4,128)S(1)}, f32[4,512,64]{1,2,0:T(8,128)S(1)}) %tuple.42, (s32[]{:T(128)}, s32[]{:T(128)}, bf16[2,1024,256]{1,2,0:T(8,128)(2,1)S(1)}, ...), branch_computations={%region_1.1_spmd, %region_2.4_spmd} | conditional | flops 577508864 | bytes 31971410 | solution.py:87
  70.4 2.5 fusion.4
  72.9 2.9 fusion.3
  75.8 3.2 fusion.8
  79.0 0.7 dynamic_slice.31
  80.8 1.0 copy.30
  81.8 4.6 %all-to-all-start = ((bf16[8,64,256]{2,1,0:T(8,128)(2,1)}), bf16[8,64,256]{2,1,0:T(8,128)(2,1)S(1)}, u32[]{:S(2)}, u32[]{:S(2)}) async-start(bf16[8,64,256]{2,1,0:T(8,128)(2,1)} %copy.30), calls=%async_computation | async-start | bytes 524288 | tf_op jit(solution)/shard_map/all_to_all | solution.py:97
  86.9 15.4 %all-to-all-done = bf16[8,64,256]{2,1,0:T(8,128)(2,1)S(1)} async-done(((bf16[8,64,256]{2,1,0:T(8,128)(2,1)}), bf16[8,64,256]{2,1,0:T(8,128)(2,1)S(1)}, u32[]{:S(2)}, u32[]{:S(2)}) %all-to-all-start) | async-done | bytes 262176 | tf_op jit(solution)/shard_map/all_to_all | solution.py:97
  102.3 53.7 %all-gather.9.cloned.1.call-done = bf16[2048,2048]{1,0:T(8,128)(2,1)} async-done(((bf16[256,2048]{1,0:T(8,128)(2,1)}), bf16[2048,2048]{1,0:T(8,128)(2,1)}) %all-gather.9.cloned.1.call-update) | async-done | bytes 8388624 | tf_op jit(solution)/shard_map/all_gather | solution.py:100
  156.0 5.1 %multiply_reduce_fusion.1 = (f32[64]{0:T(128)S(1)}, f32[64,2048]{1,0:T(8,128)S(1)}) fusion(bf16[64,2048]{1,0:T(8,128)(2,1)S(1)} %bitcast.63, bf16[2048,2048]{1,0:T(8,128)(2,1)} %all-gather.9.cloned.1.call-done, bf16[64,2048]{1,0:T(8,128)(2,1)S(1)} %copy-done.1), kind=kOutput, calls=%fused_computation.35 | convolution fusion | flops 537657280 | bytes 9437440 | tf_op jit(solution)/shard_map/dot_general | solution.py:98
  162.1 15.3 %all_to_all.29 = bf16[4,48,2048]{2,1,0:T(8,128)(2,1)} all-to-all(bf16[4,48,2048]{2,1,0:T(8,128)(2,1)S(1)} %bitcast.62), channel_id=1, replica_groups=mesh['sp'=4,'tp'=8] {'sp'}, dimensions={0} | all-to-all | bytes 1572864 | tf_op jit(solution)/shard_map/all_to_all | solution.py:121
  177.5 61.7 %all-gather.11.cloned.1.call-done = bf16[1536,2048]{1,0:T(8,128)(2,1)} async-done(((bf16[192,2048]{1,0:T(8,128)(2,1)}), bf16[1536,2048]{1,0:T(8,128)(2,1)}) %all-gather.11.cloned.1.call-update) | async-done | bytes 6291472 | tf_op jit(solution)/shard_map/all_gather | solution.py:123
  239.3 11.4 %fusion.18 = f32[1536,896]{1,0:T(8,128)} fusion(bf16[1536,2048]{1,0:T(8,128)(2,1)} %all-gather.11.cloned.1.call-done, bf16[1,2048,896]{2,1,0:T(8,128)(2,1)} %param.23), kind=kOutput, calls=%fused_computation.25 | convolution fusion | flops 5637144576 | bytes 15466496 | tf_op jit(solution)/shard_map/dot_general | solution.py:124
  250.6 20.1 %convolution_convert_fusion = bf16[1536,2048]{1,0:T(8,128)(2,1)} fusion(bf16[1,896,2048]{2,1,0:T(8,128)(2,1)} %param.25, f32[1536,896]{1,0:T(8,128)} %fusion.18, bf16[1536,2048]{1,0:T(8,128)(2,1)} %all-gather.11.cloned.1.call-done, bf16[1,2048,896]{2,1,0:T(8,128)(2,1)} %param.24), kind=kOutput, calls=%fused_computation.21 | convolution fusion | flops 11285692416 | bytes 25427968 | tf_op jit(solution)/shard_map/dot_general | solution.py:128
  270.7 68.5 %reduce-scatter.2.cloned.1.call-done = bf16[192,2048]{1,0:T(8,128)(2,1)} async-done(((bf16[1536,2048]{1,0:T(8,128)(2,1)}), bf16[192,2048]{1,0:T(8,128)(2,1)}) %reduce-scatter.2.cloned.1.call-update) | async-done | bytes 786448 | tf_op jit(solution)/shard_map/reduce_scatter | solution.py:127
  339.2 3.7 %all-to-all-start.2 = ((bf16[4,48,2048]{2,1,0:T(8,128)(2,1)}), bf16[4,48,2048]{2,1,0:T(8,128)(2,1)S(1)}, u32[]{:S(2)}, u32[]{:S(2)}) async-start(bf16[4,48,2048]{2,1,0:T(8,128)(2,1)} %bitcast.67), calls=%async_computation.3 | async-start | bytes 1572864 | tf_op jit(solution)/shard_map/all_to_all | solution.py:134
  343.3 8.7 %all-to-all-done.2 = bf16[4,48,2048]{2,1,0:T(8,128)(2,1)S(1)} async-done(((bf16[4,48,2048]{2,1,0:T(8,128)(2,1)}), bf16[4,48,2048]{2,1,0:T(8,128)(2,1)S(1)}, u32[]{:S(2)}, u32[]{:S(2)}) %all-to-all-start.2) | async-done | bytes 786464 | tf_op jit(solution)/shard_map/all_to_all | solution.py:134
  352.0 0.9 gather_fusion
  353.6 1.5 multiply_reduce_fusion
  355.1 0.8 add_convert_fusion
  (52 shorter events, 3.7 us)
Async XLA Ops:
  6.5 61.8 %copy-start = (f32[512,4]{0,1:T(4,128)S(1)}, f32[512,4]{0,1:T(4,128)}, u32[]{:S(2)}) copy-start(f32[512,4]{0,1:T(4,128)} %param.20) | copy-start | bytes 24580
  6.5 31.9 %all-gather.5.cloned.1.call-start = ((), (), s32[]{:S(2)}) async-start(), calls=%async_computation.4 | async-start | bytes 1310720 | tf_op jit(solution)/shard_map/all_gather | solution.py:69
  7.3 59.5 %all-gather.7.cloned.1.call-start = ((), (), s32[]{:S(2)}) async-start(), calls=%async_computation.5 | async-start | bytes 1310720 | tf_op jit(solution)/shard_map/all_gather | solution.py:70
  8.0 148.0 %all-gather.9.cloned.1.call-start = ((), (), s32[]{:S(2)}) async-start(), calls=%async_computation.6 | async-start | bytes 9437184 | tf_op jit(solution)/shard_map/all_gather | solution.py:100
  68.4 87.6 %copy-start.1 = (bf16[64,2048]{1,0:T(8,128)(2,1)S(1)}, bf16[64,2048]{1,0:T(8,128)(2,1)}, u32[]{:S(2)}) copy-start(bf16[64,2048]{1,0:T(8,128)(2,1)} %param.16) | copy-start | bytes 786436
  81.8 20.5 %all-to-all-start = ((bf16[8,64,256]{2,1,0:T(8,128)(2,1)}), bf16[8,64,256]{2,1,0:T(8,128)(2,1)S(1)}, u32[]{:S(2)}, u32[]{:S(2)}) async-start(bf16[8,64,256]{2,1,0:T(8,128)(2,1)} %copy.30), calls=%async_computation | async-start | bytes 524288 | tf_op jit(solution)/shard_map/all_to_all | solution.py:97
  86.4 152.9 %all-gather.11.cloned.1.call-start = ((), (), s32[]{:S(2)}) async-start(), calls=%async_computation.7 | async-start | bytes 7077888 | tf_op jit(solution)/shard_map/all_gather | solution.py:123
  156.0 5.1 %copy-start.2 = (f32[2048]{0:T(1024)S(1)}, f32[2048]{0:T(1024)}, u32[]{:S(2)}) copy-start(f32[2048]{0:T(1024)} %param.22) | copy-start | bytes 24580
  177.5 161.8 %reduce-scatter.2.cloned.1.call-start = ((), (), s32[]{:S(2)}) async-start(), calls=%async_computation.8 | async-start | bytes 7077888 | tf_op jit(solution)/shard_map/reduce_scatter | solution.py:127
  270.7 72.2 %copy-start.3 = (s32[64,2]{0,1:T(2,128)S(1)}, s32[64,2]{0,1:T(2,128)}, u32[]{:S(2)}) copy-start(s32[64,2]{0,1:T(2,128)} %param.26) | copy-start | bytes 1540
  270.7 72.5 %copy-start.4 = (f32[64,2]{0,1:T(2,128)S(1)}, f32[64,2]{0,1:T(2,128)}, u32[]{:S(2)}) copy-start(f32[64,2]{0,1:T(2,128)} %param.27) | copy-start | bytes 1540
  339.2 12.8 %all-to-all-start.2 = ((bf16[4,48,2048]{2,1,0:T(8,128)(2,1)}), bf16[4,48,2048]{2,1,0:T(8,128)(2,1)S(1)}, u32[]{:S(2)}, u32[]{:S(2)}) async-start(bf16[4,48,2048]{2,1,0:T(8,128)(2,1)} %bitcast.67), calls=%async_computation.3 | async-start | bytes 1572864 | tf_op jit(solution)/shard_map/all_to_all | solution.py:134
Sparse Core Ops, SparseCore 0:
  9.2 29.2 all-gather.4
  40.3 26.4 all-gather.6
  68.4 87.5 all-gather.8
  177.6 61.6 all-gather.10
  270.8 68.3 reduce-scatter.1
where the time goes:
time: 363 us; the launch traced here: 362 us
  waiting for transfers between devices  255 us (70%)
  matrix products  42.6 us (12%)
  blocking collectives  25.1 us (7%)
  between operations  13.4 us (4%)
  local copies, waits for them, and re-layouts  10.3 us (3%)
  starting transfers between devices  8.43 us (2%)
  other arithmetic  6.2 us (2%)
    reduce_scatter x1, waiting for transfers between devices, shards(): lax.psum_scatter(jnp.dot(hidden, down_weight[0], preferred_element_type=j...  68.5 us
    all_gather x1, waiting for transfers between devices, shards(): rows_in = lax.all_gather(row_block, 'tp', axis=0, tiled=True)  61.7 us
    all_gather x1, waiting for transfers between devices, shards(): lax.all_gather(out_weight, 'tp', axis=0, tiled=True)  53.7 us
    all_gather x1, waiting for transfers between devices, shards(): value_piece = lax.all_gather(value_vectors, 'sp', axis=0, tiled=True)  26.9 us
    dot_general x1, matrix products, shards(): jnp.dot(hidden, down_weight[0], preferred_element_type=jnp.float32)  20.1 us
    all_gather x1, waiting for transfers between devices, shards(): key_piece = lax.all_gather(key_vectors, 'sp', axis=0, tiled=True)  17.9 us
    all_to_all x1, waiting for transfers between devices, shards(): lax.all_to_all(attended, 'tp', split_axis=0, concat_axis=1, tiled=True)  15.4 us
    all_to_all x1, blocking collectives, shards(): lax.all_to_all(dispatch, 'sp', split_axis=0, concat_axis=0, tiled=True)  15.3 us
  transfers between devices with their start and end apart: 7, of which 7 were waited for; matrix products, arithmetic and copies ran while one was open for 5% of the time, Pallas kernels for 0%

commit v1 on v0

--- a/solution.py
+++ b/solution.py
@@ -66,8 +66,13 @@
         jnp.zeros((heads_here, seg_rows, head_width), jnp.float32),
     )
     carried = start_state
-    key_piece = lax.all_gather(key_vectors, "sp", axis=0, tiled=True)
-    value_piece = lax.all_gather(value_vectors, "sp", axis=0, tiled=True)
+    key_piece, value_piece = jnp.split(
+        lax.all_gather(
+            jnp.concatenate([key_vectors, value_vectors], axis=1), "sp", axis=0, tiled=True
+        ),
+        [key_vectors.shape[1]],
+        axis=1,
+    )
     row_count = key_piece.shape[0]
     block_rows = math.gcd(row_count, 1024)
     block_count = row_count // block_rows

time: 363 us -> 343 us (0.945)
  waiting for transfers between devices: 255 us -> 234 us
    all_gather x2 -> x1, waiting for transfers between devices: 44.7 us -> 26.1 us  [shards(): lax.all_gather(jnp.concatenate([key_vectors, value_vectors], axis=1), 'sp...]
    all_gather x1, waiting for transfers between devices: 53.7 us -> 49.9 us  [shards(): lax.all_gather(out_weight, 'tp', axis=0, tiled=True)]
  transfers between devices with their start and end apart: 7 -> 6, of which waited for: 7 -> 6; matrix products, arithmetic and copies ran while one was open for 5% -> 5% of each run, Pallas kernels for 0% -> 0%
where the time goes in v1:
time: 343 us
  waiting for transfers between devices  234 us (68%)
  matrix products  42.5 us (12%)
  blocking collectives  25.1 us (7%)
  between operations  13.3 us (4%)
  local copies, waits for them, and re-layouts  10 us (3%)
  starting transfers between devices  8.57 us (2%)
  other arithmetic  8.07 us (2%)
    reduce_scatter x1, waiting for transfers between devices, shards(): lax.psum_scatter(jnp.dot(hidden, down_weight[0], preferred_element_type=j...  68.5 us
    all_gather x1, waiting for transfers between devices, shards(): rows_in = lax.all_gather(row_block, 'tp', axis=0, tiled=True)  61.8 us
    all_gather x1, waiting for transfers between devices, shards(): lax.all_gather(out_weight, 'tp', axis=0, tiled=True)  49.9 us
    all_gather x1, waiting for transfers between devices, shards(): lax.all_gather(jnp.concatenate([key_vectors, value_vectors], axis=1), 'sp...  26.1 us
    dot_general x1, matrix products, shards(): jnp.dot(hidden, down_weight[0], preferred_element_type=jnp.float32)  20.1 us
    all_to_all x1, waiting for transfers between devices, shards(): lax.all_to_all(attended, 'tp', split_axis=0, concat_axis=1, tiled=True)  18 us
    all_to_all x1, blocking collectives, shards(): lax.all_to_all(dispatch, 'sp', split_axis=0, concat_axis=0, tiled=True)  15.3 us
    dot_general x1, matrix products, shards(): jnp.dot(rows_in, gate_weight[0], preferred_element_type=jnp.float32)  11.3 us
  transfers between devices with their start and end apart: 6, of which 6 were waited for; matrix products, arithmetic and copies ran while one was open for 5% of the time, Pallas kernels for 0%

profile of v1, /device:TPU:0, one launch (start us, length us, event | category | flops | bytes accessed | tf_op | source)
XLA Modules:
  0.0 342.7 jit_solution(6571135518029635389)
XLA Ops:
  6.5 1.9 pad_maximum_fusion
  8.5 0.7 all-gather.6.cloned.1.call-update
  9.2 1.1 copy.27
  10.3 0.8 copy.32
  11.2 9.8 %all_gather.13 = f32[2048,4]{0,1:T(4,128)S(1)} all-gather(f32[512,4]{0,1:T(4,128)} %param.20), channel_id=1, replica_groups=mesh['sp'=4,'tp'=8] {'sp'}, dimensions={0}, use_global_device_ids=true | all-gather | bytes 40960 | tf_op jit(solution)/shard_map/all_gather | solution.py:34
  21.0 26.1 %all-gather.4.cloned.1.call-done = bf16[2048,512]{1,0:T(8,128)(2,1)} async-done(((bf16[512,512]{1,0:T(8,128)(2,1)}), bf16[2048,512]{1,0:T(8,128)(2,1)}) %all-gather.4.cloned.1.call-update) | async-done | bytes 2097168 | tf_op jit(solution)/shard_map/all_gather | solution.py:70
  47.1 1.7 fusion.28
  48.8 0.5 copy.28
  49.3 0.5 copy.29
  50.0 11.8 %while.15 = (s32[]{:T(128)}, f32[4,512]{1,0:T(4,128)S(1)}, f32[4,512]{1,0:T(4,128)S(1)}, f32[4,512,64]{1,2,0:T(8,128)S(1)}, s32[2]{0:T(128)S(1)}, /*index=5*/s32...) while((s32[]{:T(128)}, f32[4,512]{1,0:T(4,128)S(1)}, ...), condition=%wide.region_5.6_spmd.clone, body=%wide.region_0.5_spmd.clone.sunk | while | flops 577508864 | bytes 31973748 | solution.py:94
  50.0 0.6 dynamic_slice.31
  51.3 9.2 %conditional.3 = ((f32[4,512]{1,0:T(4,128)S(1)}, f32[4,512]{1,0:T(4,128)S(1)}, f32[4,512,64]{1,2,0:T(8,128)S(1)})) conditional(s32[]{:T(128)} %convert_element_type.83, (f32[4,512]{1,0:T(4,128)S(1)}, f32[4,512]{1,0:T(4,128)S(1)}, f32[4,512,64]{1,2,0:T(8,128)S(1)}) %tuple.43, (s32[]{:T(128)}, s32[]{:T(128)}, bf16[2,1024,256]{1,2,0:T(8,128)(2,1)S(1)}, ...), branch_computations={%region_1.1_spmd, %region_2.4_spmd} | conditional | flops 577508864 | bytes 31971410 | solution.py:92
  51.9 2.5 fusion.4
  54.4 2.9 fusion.3
  57.3 3.1 fusion.8
  60.5 0.6 dynamic_slice.31
  62.1 1.0 copy.30
  63.2 4.6 %all-to-all-start = ((bf16[8,64,256]{2,1,0:T(8,128)(2,1)}), bf16[8,64,256]{2,1,0:T(8,128)(2,1)S(1)}, u32[]{:S(2)}, u32[]{:S(2)}) async-start(bf16[8,64,256]{2,1,0:T(8,128)(2,1)} %copy.30), calls=%async_computation | async-start | bytes 524288 | tf_op jit(solution)/shard_map/all_to_all | solution.py:102
  68.4 18.0 %all-to-all-done = bf16[8,64,256]{2,1,0:T(8,128)(2,1)S(1)} async-done(((bf16[8,64,256]{2,1,0:T(8,128)(2,1)}), bf16[8,64,256]{2,1,0:T(8,128)(2,1)S(1)}, u32[]{:S(2)}, u32[]{:S(2)}) %all-to-all-start) | async-done | bytes 262176 | tf_op jit(solution)/shard_map/all_to_all | solution.py:102
  86.4 49.9 %all-gather.6.cloned.1.call-done = bf16[2048,2048]{1,0:T(8,128)(2,1)} async-done(((bf16[256,2048]{1,0:T(8,128)(2,1)}), bf16[2048,2048]{1,0:T(8,128)(2,1)}) %all-gather.6.cloned.1.call-update) | async-done | bytes 8388624 | tf_op jit(solution)/shard_map/all_gather | solution.py:105
  136.3 5.1 %multiply_reduce_fusion.1 = (f32[64]{0:T(128)S(1)}, f32[64,2048]{1,0:T(8,128)S(1)}) fusion(bf16[64,2048]{1,0:T(8,128)(2,1)S(1)} %bitcast.65, bf16[2048,2048]{1,0:T(8,128)(2,1)} %all-gather.6.cloned.1.call-done, bf16[64,2048]{1,0:T(8,128)(2,1)S(1)} %copy-done.1), kind=kOutput, calls=%fused_computation.36 | convolution fusion | flops 537657280 | bytes 9437440 | tf_op jit(solution)/shard_map/dot_general | solution.py:103
  142.4 15.3 %all_to_all.29 = bf16[4,48,2048]{2,1,0:T(8,128)(2,1)} all-to-all(bf16[4,48,2048]{2,1,0:T(8,128)(2,1)S(1)} %bitcast.64), channel_id=1, replica_groups=mesh['sp'=4,'tp'=8] {'sp'}, dimensions={0} | all-to-all | bytes 1572864 | tf_op jit(solution)/shard_map/all_to_all | solution.py:126
  157.8 61.8 %all-gather.8.cloned.1.call-done = bf16[1536,2048]{1,0:T(8,128)(2,1)} async-done(((bf16[192,2048]{1,0:T(8,128)(2,1)}), bf16[1536,2048]{1,0:T(8,128)(2,1)}) %all-gather.8.cloned.1.call-update) | async-done | bytes 6291472 | tf_op jit(solution)/shard_map/all_gather | solution.py:128
  219.5 11.3 %fusion.18 = f32[1536,896]{1,0:T(8,128)} fusion(bf16[1536,2048]{1,0:T(8,128)(2,1)} %all-gather.8.cloned.1.call-done, bf16[1,2048,896]{2,1,0:T(8,128)(2,1)} %param.23), kind=kOutput, calls=%fused_computation.25 | convolution fusion | flops 5637144576 | bytes 15466496 | tf_op jit(solution)/shard_map/dot_general | solution.py:129
  230.9 20.1 %convolution_convert_fusion = bf16[1536,2048]{1,0:T(8,128)(2,1)} fusion(bf16[1,896,2048]{2,1,0:T(8,128)(2,1)} %param.25, f32[1536,896]{1,0:T(8,128)} %fusion.18, bf16[1536,2048]{1,0:T(8,128)(2,1)} %all-gather.8.cloned.1.call-done, bf16[1,2048,896]{2,1,0:T(8,128)(2,1)} %param.24), kind=kOutput, calls=%fused_computation.21 | convolution fusion | flops 11285692416 | bytes 25427968 | tf_op jit(solution)/shard_map/dot_general | solution.py:133
  251.0 68.5 %reduce-scatter.2.cloned.1.call-done = bf16[192,2048]{1,0:T(8,128)(2,1)} async-done(((bf16[1536,2048]{1,0:T(8,128)(2,1)}), bf16[192,2048]{1,0:T(8,128)(2,1)}) %reduce-scatter.2.cloned.1.call-update) | async-done | bytes 786448 | tf_op jit(solution)/shard_map/reduce_scatter | solution.py:132
  319.5 3.7 %all-to-all-start.2 = ((bf16[4,48,2048]{2,1,0:T(8,128)(2,1)}), bf16[4,48,2048]{2,1,0:T(8,128)(2,1)S(1)}, u32[]{:S(2)}, u32[]{:S(2)}) async-start(bf16[4,48,2048]{2,1,0:T(8,128)(2,1)} %bitcast.67), calls=%async_computation.3 | async-start | bytes 1572864 | tf_op jit(solution)/shard_map/all_to_all | solution.py:139
  323.6 8.7 %all-to-all-done.2 = bf16[4,48,2048]{2,1,0:T(8,128)(2,1)S(1)} async-done(((bf16[4,48,2048]{2,1,0:T(8,128)(2,1)}), bf16[4,48,2048]{2,1,0:T(8,128)(2,1)S(1)}, u32[]{:S(2)}, u32[]{:S(2)}) %all-to-all-start.2) | async-done | bytes 786464 | tf_op jit(solution)/shard_map/all_to_all | solution.py:139
  332.3 0.9 gather_fusion
  333.2 0.7 reshape.144
  333.9 1.5 multiply_reduce_fusion
  335.4 0.8 add_convert_fusion
  (51 shorter events, 3.2 us)
Async XLA Ops:
  6.5 43.4 %copy-start = (f32[512,4]{0,1:T(4,128)S(1)}, f32[512,4]{0,1:T(4,128)}, u32[]{:S(2)}) copy-start(f32[512,4]{0,1:T(4,128)} %param.20) | copy-start | bytes 24580
  6.5 40.6 %all-gather.4.cloned.1.call-start = ((), (), s32[]{:S(2)}) async-start(), calls=%async_computation.4 | async-start | bytes 2621440 | tf_op jit(solution)/shard_map/all_gather | solution.py:70
  8.5 127.9 %all-gather.6.cloned.1.call-start = ((), (), s32[]{:S(2)}) async-start(), calls=%async_computation.5 | async-start | bytes 9437184 | tf_op jit(solution)/shard_map/all_gather | solution.py:105
  50.0 86.3 %copy-start.1 = (bf16[64,2048]{1,0:T(8,128)(2,1)S(1)}, bf16[64,2048]{1,0:T(8,128)(2,1)}, u32[]{:S(2)}) copy-start(bf16[64,2048]{1,0:T(8,128)(2,1)} %param.16) | copy-start | bytes 786436
  63.2 23.3 %all-to-all-start = ((bf16[8,64,256]{2,1,0:T(8,128)(2,1)}), bf16[8,64,256]{2,1,0:T(8,128)(2,1)S(1)}, u32[]{:S(2)}, u32[]{:S(2)}) async-start(bf16[8,64,256]{2,1,0:T(8,128)(2,1)} %copy.30), calls=%async_computation | async-start | bytes 524288 | tf_op jit(solution)/shard_map/all_to_all | solution.py:102
  67.8 151.8 %all-gather.8.cloned.1.call-start = ((), (), s32[]{:S(2)}) async-start(), calls=%async_computation.6 | async-start | bytes 7077888 | tf_op jit(solution)/shard_map/all_gather | solution.py:128
  136.3 5.1 %copy-start.2 = (f32[2048]{0:T(1024)S(1)}, f32[2048]{0:T(1024)}, u32[]{:S(2)}) copy-start(f32[2048]{0:T(1024)} %param.22) | copy-start | bytes 24580
  157.7 161.8 %reduce-scatter.2.cloned.1.call-start = ((), (), s32[]{:S(2)}) async-start(), calls=%async_computation.7 | async-start | bytes 7077888 | tf_op jit(solution)/shard_map/reduce_scatter | solution.py:132
  251.0 72.2 %copy-start.3 = (s32[64,2]{0,1:T(2,128)S(1)}, s32[64,2]{0,1:T(2,128)}, u32[]{:S(2)}) copy-start(s32[64,2]{0,1:T(2,128)} %param.26) | copy-start | bytes 1540
  251.0 72.5 %copy-start.4 = (f32[64,2]{0,1:T(2,128)S(1)}, f32[64,2]{0,1:T(2,128)}, u32[]{:S(2)}) copy-start(f32[64,2]{0,1:T(2,128)} %param.27) | copy-start | bytes 1540
  319.5 12.8 %all-to-all-start.2 = ((bf16[4,48,2048]{2,1,0:T(8,128)(2,1)}), bf16[4,48,2048]{2,1,0:T(8,128)(2,1)S(1)}, u32[]{:S(2)}, u32[]{:S(2)}) async-start(bf16[4,48,2048]{2,1,0:T(8,128)(2,1)} %bitcast.67), calls=%async_computation.3 | async-start | bytes 1572864 | tf_op jit(solution)/shard_map/all_to_all | solution.py:139
Sparse Core Ops, SparseCore 0:
  9.2 37.8 all-gather.3
  48.7 87.5 all-gather.5
  157.9 61.6 all-gather.7
  251.1 68.3 reduce-scatter.1
